TPU v7x, 32 devices: a whole 2x2x4 slice. The times are simulated.
32 devices in a mesh: sp: 8 (over z, y), tp: 4 (over x, core).
Axes of the slice: x: 2, y: 2, z: 4, core: 2. Of those that a mesh axis runs over, the one named last changes fastest.
Arguments:
- tokens: bfloat16 [1024, 2048], P('sp', 'tp'), may hold values from -28 to 28
- norm_gain: bfloat16 [1, 2048], P(None, 'tp'), may hold values from 0.099609375 to 1.8984375
- conv_b_w: bfloat16 [2048, 1024], P(None, 'tp'), may hold values from -0.125 to 0.125
- conv_c_w: bfloat16 [2048, 1024], P(None, 'tp'), may hold values from -0.125 to 0.125
- conv_u_w: bfloat16 [2048, 1024], P(None, 'tp'), may hold values from -0.125 to 0.125
- conv_taps: bfloat16 [3, 1024], P(None, 'tp'), may hold values from -3.5 to 3.5
- query_w: bfloat16 [2048, 2048], P(None, 'tp'), may hold values from -0.125 to 0.125
- key_w: bfloat16 [2048, 2048], P(None, 'tp'), may hold values from -0.125 to 0.125
- value_w: bfloat16 [2048, 2048], P(None, 'tp'), may hold values from -0.125 to 0.125
- outgate_w: bfloat16 [2048, 2048], P(None, 'tp'), may hold values from -0.125 to 0.125
- gate_w: bfloat16 [2048, 2, 8], P(None, None, 'tp'), may hold values from -0.125 to 0.125
- gate_bias: float32 [2, 8], P(None, 'tp'), may hold values from -5 to 150
- mem_gain: bfloat16 [2048], P('tp'), may hold values from 0.099609375 to 1.8984375
- conv_out_w: bfloat16 [1024, 2048], P('tp'), may hold values from -0.1875 to 0.1875
- mem_out_w: bfloat16 [2048, 2048], P('tp'), may hold values from -0.125 to 0.125
Outputs:
- layer_out: bfloat16 [1024, 2048], P(('sp', 'tp'))
All inputs are finite; a program needn't handle non-finite values.
Results may differ from a plain program's by a relative error of at most 0.014.
The roundings to bfloat16 on the way count: a program that leaves them out, or rounds other values in their place, can miss the bound.
Values may be sent and summed in bfloat16 or wider, within the bound.
A program may use at most 64 MiB of HBM per device.

v0:
```python
import jax
import jax.numpy as jnp
from jax import lax
from jax.sharding import PartitionSpec as P

HEAD_DIM = 256
BLOCK = 128
MDIM = 2048
EPS = 1e-06
LOWEST = -1e30
HIGH = lax.Precision.HIGHEST


def shifted(value, axis, by):
    count = lax.axis_size(axis)
    pairs = [(i, i + by) for i in range(count) if 0 <= i + by < count]
    return lax.ppermute(value, axis, pairs)


def prefix(value, axis, join, neutral):
    count, mine = (lax.axis_size(axis), lax.axis_index(axis))
    pieces = jax.tree.map(lambda part: lax.all_gather(part, axis), value)
    total = jax.tree.map(
        lambda part, zero: jnp.full_like(part, 0) + jnp.asarray(zero, part.dtype), value, neutral
    )

    def prefix_step(position, total):
        longer = join(total, jax.tree.map(lambda part: part[position], pieces))
        return jax.tree.map(lambda new, old: jnp.where(position < mine, new, old), longer, total)

    return lax.fori_loop(0, count - 1, prefix_step, total)


def local_pass(queries, keys, values, input_pre, log_forget):
    count, width = queries.shape
    blocks = count // BLOCK

    def local_step(carry, inputs):
        memory, normer, stabil, decay_sum = carry
        query_block, key_block, value_block, input_gate, forget_block = inputs
        causal = jnp.tril(jnp.ones((BLOCK, BLOCK), dtype=bool))
        running = jnp.cumsum(forget_block)
        decays = jnp.where(
            causal, running[:, None] - running[None, :] + input_gate[None, :], -jnp.inf
        )
        inter = running + stabil
        row_max = jnp.maximum(inter, jnp.max(decays, axis=1))
        weights = jnp.exp(decays - row_max[:, None])
        scores = jnp.dot(query_block, key_block.T, precision=HIGH) * weights
        carried = jnp.exp(inter - row_max)
        numer_part = carried[:, None] * jnp.dot(query_block, memory, precision=HIGH) + jnp.dot(
            scores, value_block, precision=HIGH
        )
        denom_part = carried * jnp.dot(query_block, normer, precision=HIGH) + jnp.sum(
            scores, axis=1
        )
        new_stabil = row_max[-1]
        key_weight = jnp.exp(running[-1] - running + input_gate - new_stabil)
        fade = jnp.exp(running[-1] + stabil - new_stabil)
        memory = fade * memory + jnp.dot(
            (key_weight[:, None] * key_block).T, value_block, precision=HIGH
        )
        normer = fade * normer + jnp.dot(key_weight, key_block, precision=HIGH)
        outputs = (numer_part, denom_part, row_max, decay_sum + running)
        return ((memory, normer, new_stabil, decay_sum + running[-1]), outputs)

    inputs = (
        queries.reshape(blocks, BLOCK, width),
        keys.reshape(blocks, BLOCK, width),
        values.reshape(blocks, BLOCK, width),
        input_pre.reshape(blocks, BLOCK),
        log_forget.reshape(blocks, BLOCK),
    )
    start = (
        jnp.zeros((width, width), jnp.float32),
        jnp.zeros((width,), jnp.float32),
        jnp.zeros((), jnp.float32),
        jnp.zeros((), jnp.float32),
    )
    final, rows = lax.scan(local_step, start, inputs)
    memory, normer, stabil, decay_sum = final
    numer_rows, denom_rows, row_max, row_decay = rows
    return (
        numer_rows.reshape(count, width),
        denom_rows.reshape(count),
        row_max.reshape(count),
        row_decay.reshape(count),
        decay_sum,
        stabil,
        memory,
        normer,
    )


def finish(queries, numer_rows, denom_rows, row_max, row_decay, stabil_in, memory_in, normer_in):
    from_before = jnp.dot(queries, memory_in, precision=HIGH)
    normer_before = jnp.dot(queries, normer_in, precision=HIGH)
    top = jnp.maximum(row_max, row_decay + stabil_in)
    own_scale = jnp.exp(row_max - top)
    past_scale = jnp.exp(row_decay + stabil_in - top)
    numer_all = own_scale[:, None] * numer_rows + past_scale[:, None] * from_before
    denom_all = own_scale * denom_rows + past_scale * normer_before
    return numer_all / jnp.maximum(jnp.abs(denom_all), jnp.exp(-top))[:, None]


def join_state(earlier, later):
    sum_early, stab_early, mem_early, norm_early = earlier[:4]
    sum_late, stab_late, mem_late, norm_late = later[:4]
    top = jnp.maximum(sum_late + stab_early, stab_late)
    early_scale = jnp.exp(sum_late + stab_early - top)
    late_scale = jnp.exp(stab_late - top)
    joined = (
        sum_early + sum_late,
        top,
        early_scale[:, None, None] * mem_early + late_scale[:, None, None] * mem_late,
        early_scale[:, None] * norm_early + late_scale[:, None] * norm_late,
    )
    if len(earlier) > 4:
        edge = jnp.where(later[5][0] > 0, later[4], earlier[4])
        joined = joined + (edge, jnp.maximum(earlier[5], later[5]))
    return joined


def body(
    tokens,
    norm_gain,
    conv_b_w,
    conv_c_w,
    conv_u_w,
    conv_taps,
    query_w,
    key_w,
    value_w,
    outgate_w,
    gate_w,
    gate_bias,
    mem_gain,
    conv_out_w,
    mem_out_w,
):
    count = tokens.shape[0]
    model = conv_b_w.shape[0]
    weights = (
        conv_b_w,
        conv_c_w,
        conv_u_w,
        query_w,
        key_w,
        value_w,
        outgate_w,
        gate_w.reshape(model, -1),
    )
    piece = lax.all_gather(tokens, "tp", axis=1, tiled=True)
    gain_piece = lax.all_gather(norm_gain, "tp", axis=1, tiled=True)
    wide = piece.astype(jnp.float32)
    scaled = (wide * gain_piece.astype(jnp.float32)).astype(jnp.bfloat16)
    squares = jnp.sum(wide * wide, axis=1)
    totals = tuple(
        (jnp.dot(scaled, weight, preferred_element_type=jnp.float32) for weight in weights)
    )
    folded = (squares,) + totals
    inv_rms = lax.rsqrt(folded[0] / model + EPS)[:, None]

    def project(total):
        return lax.optimization_barrier((inv_rms * total).astype(jnp.bfloat16)).astype(jnp.float32)

    gate_b, gate_c, gate_u, queries, keys, values, outgate = [
        project(total) for total in folded[1:8]
    ]
    heads = gate_bias.shape[1]
    gates = inv_rms * folded[8]
    input_pre = gates[:, :heads] + gate_bias[0]
    forget_pre = gates[:, heads:] + gate_bias[1]
    mixed_in = (gate_c * gate_u).astype(jnp.bfloat16)
    reach = conv_taps.shape[0] - 1
    head_q = queries.reshape(count, heads, HEAD_DIM)
    head_k = keys.reshape(count, heads, HEAD_DIM) * HEAD_DIM ** (-0.5)
    head_v = values.reshape(count, heads, HEAD_DIM)
    local = jax.vmap(local_pass, in_axes=1, out_axes=(1, 1, 1, 1, 0, 0, 0, 0))(
        head_q, head_k, head_v, input_pre, jax.nn.log_sigmoid(forget_pre)
    )
    numer_rows, denom_rows, row_max, row_decay, decay_sum, stabil, memory, normer = local
    identity = (
        jnp.zeros((heads,), jnp.float32),
        jnp.full((heads,), LOWEST, jnp.float32),
        jnp.zeros((heads, HEAD_DIM, HEAD_DIM), jnp.float32),
        jnp.zeros((heads, HEAD_DIM), jnp.float32),
    )
    before = shifted(mixed_in[count - reach :], "sp", 1)
    incoming = prefix((decay_sum, stabil, memory, normer), "sp", join_state, identity)
    padded = jnp.concatenate([before, mixed_in], axis=0).astype(jnp.float32)
    taps = conv_taps.astype(jnp.float32)
    conv_sum = taps[0] * padded[0:count]
    for offset in range(1, reach + 1):
        conv_sum = conv_sum + taps[offset] * padded[offset : offset + count]
    y_conv = (gate_b * conv_sum).astype(jnp.bfloat16)
    mem_raw = jax.vmap(finish, in_axes=(1, 1, 1, 1, 1, 0, 0, 0), out_axes=1)(
        head_q, numer_rows, denom_rows, row_max, row_decay, incoming[1], incoming[2], incoming[3]
    )
    flat_raw = mem_raw.reshape(count, -1)
    own_squares = jnp.sum(flat_raw * flat_raw, axis=1)
    all_squares = lax.psum(own_squares, "tp")
    mem_norm = flat_raw * lax.rsqrt(all_squares / MDIM + EPS)[:, None]
    mem_norm = mem_norm * mem_gain.astype(jnp.float32)[None, :]
    y_mem = (jax.nn.sigmoid(outgate) * mem_norm).astype(jnp.bfloat16)
    return lax.psum_scatter(
        (
            jnp.dot(y_conv, conv_out_w, preferred_element_type=jnp.float32)
            + jnp.dot(y_mem, mem_out_w, preferred_element_type=jnp.float32)
        ).astype(jnp.bfloat16),
        "tp",
        scatter_dimension=0,
        tiled=True,
    )


def solution(mesh):
    return jax.shard_map(
        body,
        mesh=mesh,
        in_specs=(
            P("sp", "tp"),
            P(None, "tp"),
            P(None, "tp"),
            P(None, "tp"),
            P(None, "tp"),
            P(None, "tp"),
            P(None, "tp"),
            P(None, "tp"),
            P(None, "tp"),
            P(None, "tp"),
            P(None, None, "tp"),
            P(None, "tp"),
            P("tp"),
            P("tp", None),
            P("tp", None),
        ),
        out_specs=P(("sp", "tp"), None),
        check_vma=False,
    )
```

profile of v0, /device:TPU:0, one launch (start us, length us, event | category | flops | bytes accessed | tf_op | source)
XLA Modules:
  0.0 148.9 jit_solution(2480114630991469454)
XLA Ops:
  6.6 0.8 slice_bitcast_fusion
  7.4 6.3 %all_gather.31 = bf16[1,2048]{1,0:T(2,128)(2,1)S(1)} all-gather(bf16[1,512]{1,0:T(2,128)(2,1)} %param.18), channel_id=1, replica_groups=mesh['sp'=8,'tp'=4] {'tp'}, dimensions={1}, use_global_device_ids=true | all-gather | bytes 5120 | tf_op jit(solution)/shard_map/all_gather | solution.py:154
  13.7 0.7 reshape.140
  14.5 7.9 %all_gather.30 = bf16[128,2048]{1,0:T(8,128)(2,1)S(1)} all-gather(bf16[128,512]{1,0:T(8,128)(2,1)} %param.17), channel_id=1, replica_groups=mesh['sp'=8,'tp'=4] {'tp'}, dimensions={1}, use_global_device_ids=true | all-gather | bytes 655360 | tf_op jit(solution)/shard_map/all_gather | solution.py:153
  22.3 0.2 fusion.21
  22.5 0.2 convolution_multiply_fusion.8
  22.9 0.3 reduce_window_sum.14
  23.2 0.1 fusion.41
  23.3 0.2 multiply_reduce_fusion.1
  23.7 2.2 %fusion.15 = bf16[128,512]{1,0:T(8,128)(2,1)S(1)} fusion(bf16[2048,512]{1,0:T(8,128)(2,1)} %param.24, f32[128]{0:T(128)S(1)} %add_rsqrt_fusion.1, bf16[128,2048]{1,0:T(8,128)(2,1)S(1)} %all_gather.30, f32[2048]{0:T(1024)S(1)} %bitcast.213), kind=kOutput, calls=%fused_computation.34 | convolution fusion | flops 269352960 | bytes 2761216 | tf_op jit(solution)/shard_map/dot_general | solution.py:159
  25.9 0.4 fusion.16
  26.4 1.3 convolution_add_fusion.1
  27.7 1.5 %fusion.19 = bf16[128,256]{1,0:T(8,128)(2,1)S(1)} fusion(bf16[2048,256]{1,0:T(8,128)(2,1)} %param.20, f32[128]{0:T(128)S(1)} %add_rsqrt_fusion.1, bf16[128,2048]{1,0:T(8,128)(2,1)S(1)} %all_gather.30, f32[2048]{0:T(1024)S(1)} %bitcast.215), kind=kOutput, calls=%fused_computation.42 | convolution fusion | flops 135069696 | bytes 1647104 | tf_op jit(solution)/shard_map/dot_general | solution.py:159
  29.3 1.5 %fusion.20 = bf16[128,256]{1,0:T(8,128)(2,1)S(1)} fusion(bf16[2048,256]{1,0:T(8,128)(2,1)} %param.21, f32[128]{0:T(128)S(1)} %add_rsqrt_fusion.1, bf16[128,2048]{1,0:T(8,128)(2,1)S(1)} %all_gather.30, f32[2048]{0:T(1024)S(1)} %bitcast.216), kind=kOutput, calls=%fused_computation.43 | convolution fusion | flops 135069696 | bytes 1647104 | tf_op jit(solution)/shard_map/dot_general | solution.py:159
  30.9 3.5 %collective-permute-start = (bf16[2,256]{1,0:T(2,128)(2,1)S(1)}, bf16[2,256]{1,0:T(2,128)(2,1)S(1)}, u32[]{:S(2)}, u32[]{:S(2)}) collective-permute-start(bf16[2,256]{1,0:T(2,128)(2,1)S(1)} %slice.57), channel_id=1, source_target_pairs={{0,4},{4,8},{8,12},{12,16},{16,20},{20,24},{24,28},{1,5},{5,9},{9,... | collective-permute-start | bytes 3080 | tf_op jit(solution)/shard_map/ppermute | solution.py:17
  34.4 0.6 dynamic-slice.10
  35.7 0.2 dynamic-update-slice
  35.9 0.2 dynamic-update-slice.1
  36.1 2.3 %fusion.17 = bf16[128,512]{1,0:T(8,128)(2,1)S(1)} fusion(bf16[2048,512]{1,0:T(8,128)(2,1)} %param.23, f32[128]{0:T(128)S(1)} %add_rsqrt_fusion.1, bf16[128,2048]{1,0:T(8,128)(2,1)S(1)} %all_gather.30, f32[2048]{0:T(1024)S(1)} %bitcast.217), kind=kOutput, calls=%fused_computation.36 | convolution fusion | flops 269352960 | bytes 2761216 | tf_op jit(solution)/shard_map/dot_general | solution.py:159
  38.4 0.2 fusion.23
  38.8 0.2 fusion.33
  38.9 0.3 fusion.80
  39.3 0.3 convolution_bitcast_fusion.2
  39.6 0.3 fusion.18
  40.0 0.4 fusion.14
  40.5 27.0 %all-gather.4 = f32[8,2,256]{2,1,0:T(2,128)S(1)} all-gather(f32[1,2,256]{2,1,0:T(2,128)S(1)} %fusion.63), channel_id=5, replica_groups=mesh['sp'=8,'tp'=4] {'sp'}, dimensions={0}, use_global_device_ids=true | all-gather | bytes 18432 | tf_op jit(solution)/shard_map/all_gather | solution.py:22
  67.5 19.8 %all-reduce.2 = (f32[16]{0:T(128)S(1)}, f32[16]{0:T(128)S(1)}) all-reduce(f32[16]{0:T(128)S(1)} %dynamic-update-slice, f32[16]{0:T(128)S(1)} %dynamic-update-slice.1), channel_id=2, replica_groups=mesh['sp'=8,'tp'=4] {'sp'}, use_global_device_ids=true, to_apply=%add | all-reduce | flops 32 | bytes 256
  87.5 2.5 %fusion.50 = f32[128,2048]{1,0:T(8,128)} fusion(bf16[256,2048]{1,0:T(8,128)(2,1)} %param.30, f32[130,256]{1,0:T(8,128)S(1)} %maximum_convert_fusion, bf16[128,256]{1,0:T(8,128)(2,1)S(1)} %fusion.18, f32[256]{0:T(256)S(1)} %bitcast.230, f32[256]{0:T(256)S(1)} %bitcast.229, f32[256]{0:T(256)S(1)} %bitcast.228), kind=kOutput, calls=%fused_computation.85 | convolution fusion | flops 134479872 | bytes 2558976 | tf_op jit(solution)/shard_map/dot_general | solution.py:208
  90.1 12.7 %all-gather.7.cloned.1.call-done = f32[16,256,256]{2,1,0:T(8,128)} async-done(((f32[2,256,256]{2,1,0:T(8,128)}), f32[16,256,256]{2,1,0:T(8,128)}) %all-gather.7.cloned.1.call-update) | async-done | bytes 4194320 | tf_op jit(solution)/shard_map/all_gather | solution.py:22
  102.8 9.3 %while.5 = (s32[]{:T(128)}, f32[2]{0:T(128)S(1)}, f32[2,256,256]{2,1,0:T(8,128)S(1)}, f32[2,256]{1,0:T(2,128)S(1)}, s32[]{:T(128)}, /*index=5*/f32[8,2]{1,0:T(8,...) while((s32[]{:T(128)}, f32[2]{0:T(128)S(1)}, ...), condition=%wide.region_4.5_spmd.clone, body=%wide.region_3.4_spmd.clone.sunk | while | flops 657940 | bytes 1579278 | solution.py:31
  102.8 0.1 fusion.97
  102.9 1.2 fusion.96
  104.2 0.1 fusion.97
  104.3 1.2 fusion.96
  105.6 1.2 fusion.96
  106.9 0.1 fusion.97
  106.9 1.2 fusion.96
  108.2 0.1 fusion.97
  108.3 1.2 fusion.96
  109.5 0.1 fusion.97
  109.6 1.2 fusion.96
  111.0 1.2 fusion.96
  112.1 0.2 fusion.31
  112.4 0.3 fusion.13
  112.7 0.5 multiply_reduce_fusion
  113.2 5.7 %psum.7 = f32[128]{0:T(128)S(1)} all-reduce(f32[128]{0:T(128)S(1)} %get-tuple-element.276), channel_id=1, replica_groups=mesh['sp'=8,'tp'=4] {'tp'}, use_global_device_ids=true, to_apply=%region_7.8 | all-reduce | flops 128 | bytes 1024 | tf_op jit(solution)/shard_map/psum | solution.py:202
  118.9 2.5 %fusion.7 = bf16[128,2048]{1,0:T(8,128)(2,1)} fusion(f32[128,2048]{1,0:T(8,128)} %fusion.50, bf16[512,2048]{1,0:T(8,128)(2,1)S(1)} %copy-done, f32[128,512]{1,0:T(8,128)S(1)} %bitcast.211, bf16[128,512]{1,0:T(8,128)(2,1)S(1)} %fusion.14, f32[512]{0:T(512)S(1)} %convert_element_type.84, f32[128]{0:T(128)S(1)} %add_rsqrt_fusion), kind=kOutput, calls=%fused_computation.16 | convolution fusion | flops 269484032 | bytes 4065792 | tf_op jit(solution)/shard_map/dot_general | solution.py:209
  121.4 20.7 %reduce-scatter.2.cloned.1.call-done = bf16[32,2048]{1,0:T(8,128)(2,1)} async-done(((bf16[128,2048]{1,0:T(8,128)(2,1)}), bf16[32,2048]{1,0:T(8,128)(2,1)}) %reduce-scatter.2.cloned.1.call-update) | async-done | bytes 131088 | tf_op jit(solution)/shard_map/reduce_scatter | solution.py:206
  (59 shorter events, 1.2 us)
Async XLA Ops:
  6.5 112.4 %copy-start = (bf16[512,2048]{1,0:T(8,128)(2,1)S(1)}, bf16[512,2048]{1,0:T(8,128)(2,1)}, u32[]{:S(2)}) copy-start(bf16[512,2048]{1,0:T(8,128)(2,1)} %param.31) | copy-start | bytes 6291460
  6.5 96.3 %all-gather.7.cloned.1.call-start = ((), (), s32[]{:S(2)}) async-start(), calls=%async_computation.2 | async-start | bytes 4718592 | tf_op jit(solution)/shard_map/all_gather | solution.py:22
  23.2 2.7 %copy-start.1 = (bf16[2048,512]{1,0:T(8,128)(2,1)S(1)}, bf16[2048,512]{1,0:T(8,128)(2,1)}, u32[]{:S(2)}) copy-start(bf16[2048,512]{1,0:T(8,128)(2,1)} %param.25) | copy-start | bytes 6291460
  27.7 6.8 %copy-start.6 = (u32[32]{0:T(128)S(1)}, u32[32]{0:T(128)}, u32[]{:S(2)}) copy-start(u32[32]{0:T(128)} %constant.86) | copy-start | bytes 388
  27.7 114.4 %reduce-scatter.2.cloned.1.call-start = ((), (), s32[]{:S(2)}) async-start(), calls=%async_computation.1 | async-start | bytes 655360 | tf_op jit(solution)/shard_map/reduce_scatter | solution.py:206
  29.3 9.5 %copy-start.4 = (bf16[3,256]{1,0:T(4,128)(2,1)S(1)}, bf16[3,256]{1,0:T(4,128)(2,1)}, u32[]{:S(2)}) copy-start(bf16[3,256]{1,0:T(4,128)(2,1)} %param.22) | copy-start | bytes 4612
  30.9 56.6 %collective-permute-start = (bf16[2,256]{1,0:T(2,128)(2,1)S(1)}, bf16[2,256]{1,0:T(2,128)(2,1)S(1)}, u32[]{:S(2)}, u32[]{:S(2)}) collective-permute-start(bf16[2,256]{1,0:T(2,128)(2,1)S(1)} %slice.57), channel_id=1, source_target_pairs={{0,4},{4,8},{8,12},{12,16},{16,20},{20,24},{24,28},{1,5},{5,9},{9,... | collective-permute-start | bytes 3080 | tf_op jit(solution)/shard_map/ppermute | solution.py:17
  36.1 3.5 %copy-start.3 = (bf16[2048,256]{1,0:T(8,128)(2,1)S(1)}, bf16[2048,256]{1,0:T(8,128)(2,1)}, u32[]{:S(2)}) copy-start(bf16[2048,256]{1,0:T(8,128)(2,1)} %param.19) | copy-start | bytes 3145732
  38.4 1.6 %copy-start.2 = (bf16[2048,512]{1,0:T(8,128)(2,1)S(1)}, bf16[2048,512]{1,0:T(8,128)(2,1)}, u32[]{:S(2)}) copy-start(bf16[2048,512]{1,0:T(8,128)(2,1)} %param.26) | copy-start | bytes 6291460
  39.6 47.7 %copy-start.5 = (bf16[512]{0:T(512)(128)(2,1)S(1)}, bf16[512]{0:T(512)(128)(2,1)}, u32[]{:S(2)}) copy-start(bf16[512]{0:T(512)(128)(2,1)} %param.29) | copy-start | bytes 3076
Sparse Core Ops, SparseCore 0:
  27.8 74.9 all-gather.6
  121.6 20.4 reduce-scatter.1
where the time goes:
time: 150 us; the launch traced here: 149 us
  blocking collectives  66.7 us (44%)
  waiting for transfers between devices  33.4 us (22%)
  matrix products  17.4 us (12%)
  between operations  14.3 us (10%)
  other arithmetic  10.4 us (7%)
  starting transfers between devices  3.57 us (2%)
  local copies, waits for them, and re-layouts  2.92 us (2%)
    all_gather x1, blocking collectives, prefix(): pieces = jax.tree.map(lambda part: lax.all_gather(part, axis), value)  27 us
    reduce_scatter x1, waiting for transfers between devices, body(): lax.psum_scatter((jnp.dot(y_conv, conv_out_w, preferred_element_type=jnp....  20.7 us
    unnamed x1, blocking collectives  19.8 us
    all_gather x1, waiting for transfers between devices, prefix(): pieces = jax.tree.map(lambda part: lax.all_gather(part, axis), value)  12.7 us
    dot_general x8, matrix products, body(): jnp.dot(scaled, weight, preferred_element_type=jnp.float32)  9 us
    select_n x14, other arithmetic, prefix_step(): jnp.where(position < mine, new, old)  8.88 us
    all_gather x1, blocking collectives, body(): piece = lax.all_gather(tokens, 'tp', axis=1, tiled=True)  7.85 us
    all_gather x1, blocking collectives, body(): gain_piece = lax.all_gather(norm_gain, 'tp', axis=1, tiled=True)  6.32 us
  transfers between devices with their start and end apart: 3, of which 2 were waited for; matrix products, arithmetic and copies ran while one was open for 7% of the time, Pallas kernels for 0%

commit v1 on v0

--- a/solution.py
+++ b/solution.py
@@ -150,7 +150,8 @@
         outgate_w,
         gate_w.reshape(model, -1),
     )
-    piece = lax.all_gather(tokens, "tp", axis=1, tiled=True)
+    parts = lax.all_gather(tokens, "tp")
+    piece = jnp.concatenate(parts, axis=1)
     gain_piece = lax.all_gather(norm_gain, "tp", axis=1, tiled=True)
     wide = piece.astype(jnp.float32)
     scaled = (wide * gain_piece.astype(jnp.float32)).astype(jnp.bfloat16)

time: 150 us -> 157 us (1.047)
  other arithmetic: 10.4 us -> 14.2 us
  local copies, waits for them, and re-layouts: 2.92 us -> 6.67 us
    convert_element_type x0 -> x2, local copies, waits for them, and re-layouts: none -> 3.9 us  [the longest x1 2.59 us: body(): wide = piece.astype(jnp.float32)]
    convert_element_type x0 -> x5, other arithmetic: none -> 3.77 us  [the longest x4 2.64 us: body(): scaled = (wide * gain_piece.astype(jnp.float32)).astype(jnp.bfloat16)]
where the time goes in v1:
time: 157 us
  blocking collectives  66.7 us (42%)
  waiting for transfers between devices  33.4 us (21%)
  matrix products  17.4 us (11%)
  between operations  14.3 us (9%)
  other arithmetic  14.2 us (9%)
  local copies, waits for them, and re-layouts  6.67 us (4%)
  starting transfers between devices  3.58 us (2%)
    all_gather x1, blocking collectives, prefix(): pieces = jax.tree.map(lambda part: lax.all_gather(part, axis), value)  27 us
    reduce_scatter x1, waiting for transfers between devices, body(): lax.psum_scatter((jnp.dot(y_conv, conv_out_w, preferred_element_type=jnp....  20.6 us
    unnamed x1, blocking collectives  19.7 us
    all_gather x1, waiting for transfers between devices, prefix(): pieces = jax.tree.map(lambda part: lax.all_gather(part, axis), value)  12.7 us
    dot_general x8, matrix products, body(): jnp.dot(scaled, weight, preferred_element_type=jnp.float32)  9.07 us
    select_n x14, other arithmetic, prefix_step(): jnp.where(position < mine, new, old)  8.88 us
    all_gather x1, blocking collectives, body(): parts = lax.all_gather(tokens, 'tp')  7.85 us
    all_gather x1, blocking collectives, body(): gain_piece = lax.all_gather(norm_gain, 'tp', axis=1, tiled=True)  6.45 us
  transfers between devices with their start and end apart: 3, of which 2 were waited for; matrix products, arithmetic and copies ran while one was open for 7% of the time, Pallas kernels for 0%

profile of v1, /device:TPU:0, one launch (start us, length us, event | category | flops | bytes accessed | tf_op | source)
XLA Modules:
  0.0 156.5 jit_solution(6566375253061000092)
XLA Ops:
  6.5 6.5 %all_gather.35 = bf16[1,2048]{1,0:T(2,128)(2,1)S(1)} all-gather(bf16[1,512]{1,0:T(2,128)(2,1)} %param.18), channel_id=1, replica_groups=mesh['sp'=8,'tp'=4] {'tp'}, dimensions={1}, use_global_device_ids=true | all-gather | bytes 5120 | tf_op jit(solution)/shard_map/all_gather | solution.py:155
  13.1 0.8 slice_bitcast_fusion
  13.8 0.7 reshape.150
  14.6 7.9 %all-gather = bf16[512,512]{1,0:T(8,128)(2,1)S(1)} all-gather(bf16[128,512]{1,0:T(8,128)(2,1)} %param.17), channel_id=2, replica_groups=mesh['sp'=8,'tp'=4] {'tp'}, dimensions={0}, use_global_device_ids=true | all-gather | bytes 655360 | tf_op jit(solution)/shard_map/all_gather | solution.py:153
  22.4 0.2 fusion.21
  22.6 0.9 fusion.24
  23.5 1.3 copy.40
  24.8 0.2 convolution_multiply_fusion.8
  25.1 0.3 reduce_window_sum.14
  25.4 0.2 fusion.43
  25.6 0.2 multiply_reduce_fusion.1
  25.9 1.1 convert_bitcast_fusion
  27.0 2.6 %copy.39 = f32[128,4,512]{0,2,1:T(8,128)} copy(f32[128,4,512]{2,0,1:T(8,128)} %convert_bitcast_fusion) | data formatting | bytes 2097152 | tf_op jit(solution)/shard_map/convert_element_type | solution.py:156
  29.6 1.7 %fusion.23 = bf16[128,2048]{0,1:T(8,128)(2,1)S(1)} fusion(f32[128,4,512]{0,2,1:T(8,128)} %copy.39, f32[2048]{0:T(1024)S(1)} %bitcast.242), kind=kLoop, calls=%fused_computation.49 | loop fusion | flops 524288 | bytes 1581056 | tf_op jit(solution)/shard_map/convert_element_type | solution.py:157
  31.3 2.1 %fusion.16 = bf16[128,512]{1,0:T(8,128)(2,1)S(1)} fusion(bf16[128,2048]{0,1:T(8,128)(2,1)S(1)} %fusion.23, bf16[2048,512]{1,0:T(8,128)(2,1)} %param.25, f32[128]{0:T(128)S(1)} %add_rsqrt_fusion.1), kind=kOutput, calls=%fused_computation.36 | convolution fusion | flops 268566528 | bytes 2753024 | tf_op jit(solution)/shard_map/dot_general | solution.py:160
  33.4 0.5 fusion.15
  33.9 1.3 convolution_add_fusion.1
  35.3 1.6 %fusion.20 = bf16[128,256]{1,0:T(8,128)(2,1)S(1)} fusion(bf16[128,2048]{0,1:T(8,128)(2,1)S(1)} %fusion.23, bf16[2048,256]{1,0:T(8,128)(2,1)} %param.21, f32[128]{0:T(128)S(1)} %add_rsqrt_fusion.1), kind=kOutput, calls=%fused_computation.44 | convolution fusion | flops 134283264 | bytes 1638912 | tf_op jit(solution)/shard_map/dot_general | solution.py:160
  36.9 1.6 %fusion.19 = bf16[128,256]{1,0:T(8,128)(2,1)S(1)} fusion(bf16[128,2048]{0,1:T(8,128)(2,1)S(1)} %fusion.23, bf16[2048,256]{1,0:T(8,128)(2,1)} %param.20, f32[128]{0:T(128)S(1)} %add_rsqrt_fusion.1), kind=kOutput, calls=%fused_computation.43 | convolution fusion | flops 134283264 | bytes 1638912 | tf_op jit(solution)/shard_map/dot_general | solution.py:160
  38.6 3.5 %collective-permute-start = (bf16[2,256]{1,0:T(2,128)(2,1)S(1)}, bf16[2,256]{1,0:T(2,128)(2,1)S(1)}, u32[]{:S(2)}, u32[]{:S(2)}) collective-permute-start(bf16[2,256]{1,0:T(2,128)(2,1)S(1)} %slice.57), channel_id=1, source_target_pairs={{0,4},{4,8},{8,12},{12,16},{16,20},{20,24},{24,28},{1,5},{5,9},{9,... | collective-permute-start | bytes 3080 | tf_op jit(solution)/shard_map/ppermute | solution.py:17
  42.1 0.6 dynamic-slice.10
  43.4 0.2 dynamic-update-slice
  43.6 0.2 dynamic-update-slice.1
  43.8 2.3 %fusion.17 = bf16[128,512]{1,0:T(8,128)(2,1)S(1)} fusion(bf16[128,2048]{0,1:T(8,128)(2,1)S(1)} %fusion.23, bf16[2048,512]{1,0:T(8,128)(2,1)} %param.23, f32[128]{0:T(128)S(1)} %add_rsqrt_fusion.1), kind=kOutput, calls=%fused_computation.37 | convolution fusion | flops 268566528 | bytes 2753024 | tf_op jit(solution)/shard_map/dot_general | solution.py:160
  46.2 0.2 fusion.25
  46.5 0.2 fusion.35
  46.7 0.3 fusion.74
  47.0 0.3 convolution_bitcast_fusion.2
  47.4 0.4 fusion.18
  47.7 0.5 fusion.14
  48.2 27.0 %all-gather.5 = f32[8,2,256]{2,1,0:T(2,128)S(1)} all-gather(f32[1,2,256]{2,1,0:T(2,128)S(1)} %fusion.57), channel_id=6, replica_groups=mesh['sp'=8,'tp'=4] {'sp'}, dimensions={0}, use_global_device_ids=true | all-gather | bytes 18432 | tf_op jit(solution)/shard_map/all_gather | solution.py:22
  75.2 19.7 %all-reduce.2 = (f32[16]{0:T(128)S(1)}, f32[16]{0:T(128)S(1)}) all-reduce(f32[16]{0:T(128)S(1)} %dynamic-update-slice, f32[16]{0:T(128)S(1)} %dynamic-update-slice.1), channel_id=3, replica_groups=mesh['sp'=8,'tp'=4] {'sp'}, use_global_device_ids=true, to_apply=%add | all-reduce | flops 32 | bytes 256
  95.2 2.5 %fusion.52 = f32[128,2048]{1,0:T(8,128)} fusion(bf16[256,2048]{1,0:T(8,128)(2,1)} %param.30, f32[130,256]{1,0:T(8,128)S(1)} %maximum_convert_fusion, bf16[128,256]{1,0:T(8,128)(2,1)S(1)} %fusion.18, f32[256]{0:T(256)S(1)} %bitcast.246, f32[256]{0:T(256)S(1)} %bitcast.245, f32[256]{0:T(256)S(1)} %bitcast.244), kind=kOutput, calls=%fused_computation.89 | convolution fusion | flops 134479872 | bytes 2558976 | tf_op jit(solution)/shard_map/dot_general | solution.py:209
  97.7 12.7 %all-gather.8.cloned.1.call-done = f32[16,256,256]{2,1,0:T(8,128)} async-done(((f32[2,256,256]{2,1,0:T(8,128)}), f32[16,256,256]{2,1,0:T(8,128)}) %all-gather.8.cloned.1.call-update) | async-done | bytes 4194320 | tf_op jit(solution)/shard_map/all_gather | solution.py:22
  110.5 9.3 %while.5 = (s32[]{:T(128)}, f32[2]{0:T(128)S(1)}, f32[2,256,256]{2,1,0:T(8,128)S(1)}, f32[2,256]{1,0:T(2,128)S(1)}, s32[]{:T(128)}, /*index=5*/f32[8,2]{1,0:T(8,...) while((s32[]{:T(128)}, f32[2]{0:T(128)S(1)}, ...), condition=%wide.region_4.5_spmd.clone, body=%wide.region_3.4_spmd.clone.sunk | while | flops 657940 | bytes 1579278 | solution.py:31
  110.6 1.2 fusion.98
  111.9 1.2 fusion.98
  113.3 1.2 fusion.98
  114.6 1.2 fusion.98
  115.9 1.2 fusion.98
  117.3 1.2 fusion.98
  118.6 1.2 fusion.98
  119.8 0.2 fusion.33
  120.1 0.3 fusion.13
  120.4 0.5 multiply_reduce_fusion
  120.8 5.7 %psum.7 = f32[128]{0:T(128)S(1)} all-reduce(f32[128]{0:T(128)S(1)} %get-tuple-element.276), channel_id=1, replica_groups=mesh['sp'=8,'tp'=4] {'tp'}, use_global_device_ids=true, to_apply=%region_7.8 | all-reduce | flops 128 | bytes 1024 | tf_op jit(solution)/shard_map/psum | solution.py:203
  126.5 2.5 %fusion.7 = bf16[128,2048]{1,0:T(8,128)(2,1)} fusion(f32[128,2048]{1,0:T(8,128)} %fusion.52, bf16[512,2048]{1,0:T(8,128)(2,1)S(1)} %copy-done, f32[128,512]{1,0:T(8,128)S(1)} %bitcast.234, bf16[128,512]{1,0:T(8,128)(2,1)S(1)} %fusion.14, f32[512]{0:T(512)S(1)} %convert_element_type.112, f32[128]{0:T(128)S(1)} %add_rsqrt_fusion), kind=kOutput, calls=%fused_computation.16 | convolution fusion | flops 269484032 | bytes 4065792 | tf_op jit(solution)/shard_map/dot_general | solution.py:210
  129.1 20.6 %reduce-scatter.2.cloned.1.call-done = bf16[32,2048]{1,0:T(8,128)(2,1)} async-done(((bf16[128,2048]{1,0:T(8,128)(2,1)}), bf16[32,2048]{1,0:T(8,128)(2,1)}) %reduce-scatter.2.cloned.1.call-update) | async-done | bytes 131088 | tf_op jit(solution)/shard_map/reduce_scatter | solution.py:207
  (66 shorter events, 1.6 us)
Async XLA Ops:
  6.5 120.0 %copy-start = (bf16[512,2048]{1,0:T(8,128)(2,1)S(1)}, bf16[512,2048]{1,0:T(8,128)(2,1)}, u32[]{:S(2)}) copy-start(bf16[512,2048]{1,0:T(8,128)(2,1)} %param.31) | copy-start | bytes 6291460
  6.5 103.9 %all-gather.8.cloned.1.call-start = ((), (), s32[]{:S(2)}) async-start(), calls=%async_computation.2 | async-start | bytes 4718592 | tf_op jit(solution)/shard_map/all_gather | solution.py:22
  29.6 3.8 %copy-start.1 = (bf16[2048,512]{1,0:T(8,128)(2,1)S(1)}, bf16[2048,512]{1,0:T(8,128)(2,1)}, u32[]{:S(2)}) copy-start(bf16[2048,512]{1,0:T(8,128)(2,1)} %param.24) | copy-start | bytes 6291460
  35.2 6.9 %copy-start.6 = (u32[32]{0:T(128)S(1)}, u32[32]{0:T(128)}, u32[]{:S(2)}) copy-start(u32[32]{0:T(128)} %constant.86) | copy-start | bytes 388
  35.3 114.4 %reduce-scatter.2.cloned.1.call-start = ((), (), s32[]{:S(2)}) async-start(), calls=%async_computation.1 | async-start | bytes 655360 | tf_op jit(solution)/shard_map/reduce_scatter | solution.py:207
  36.9 9.6 %copy-start.4 = (bf16[3,256]{1,0:T(4,128)(2,1)S(1)}, bf16[3,256]{1,0:T(4,128)(2,1)}, u32[]{:S(2)}) copy-start(bf16[3,256]{1,0:T(4,128)(2,1)} %param.22) | copy-start | bytes 4612
  38.6 56.6 %collective-permute-start = (bf16[2,256]{1,0:T(2,128)(2,1)S(1)}, bf16[2,256]{1,0:T(2,128)(2,1)S(1)}, u32[]{:S(2)}, u32[]{:S(2)}) collective-permute-start(bf16[2,256]{1,0:T(2,128)(2,1)S(1)} %slice.57), channel_id=1, source_target_pairs={{0,4},{4,8},{8,12},{12,16},{16,20},{20,24},{24,28},{1,5},{5,9},{9,... | collective-permute-start | bytes 3080 | tf_op jit(solution)/shard_map/ppermute | solution.py:17
  43.8 3.5 %copy-start.3 = (bf16[2048,256]{1,0:T(8,128)(2,1)S(1)}, bf16[2048,256]{1,0:T(8,128)(2,1)}, u32[]{:S(2)}) copy-start(bf16[2048,256]{1,0:T(8,128)(2,1)} %param.19) | copy-start | bytes 3145732
  46.1 1.6 %copy-start.2 = (bf16[2048,512]{1,0:T(8,128)(2,1)S(1)}, bf16[2048,512]{1,0:T(8,128)(2,1)}, u32[]{:S(2)}) copy-start(bf16[2048,512]{1,0:T(8,128)(2,1)} %param.26) | copy-start | bytes 6291460
  47.3 47.6 %copy-start.5 = (bf16[512]{0:T(512)(128)(2,1)S(1)}, bf16[512]{0:T(512)(128)(2,1)}, u32[]{:S(2)}) copy-start(bf16[512]{0:T(512)(128)(2,1)} %param.29) | copy-start | bytes 3076
Sparse Core Ops, SparseCore 0:
  35.4 75.0 all-gather.7
  129.2 20.4 reduce-scatter.1
